TPU v7x, 32 devices: a whole 2x2x4 slice. The times are simulated.
32 devices in a mesh: ep: 8 (over z, y), tp: 4 (over x, core).
Axes of the slice: x: 2, y: 2, z: 4, core: 2. Of those that a mesh axis runs over, the one named last changes fastest.
Arguments:
- query_rows: bfloat16 [8192, 1024], P('ep', 'tp'), may hold values from -140 to 140
- key_rows: bfloat16 [8192, 256], P('ep', 'tp'), may hold values from -4.5 to 4.5
- value_rows: bfloat16 [8192, 256], P('ep', 'tp'), may hold values from -6 to 6
- sink_logit: float32 [16], P('tp'), may hold values from 1 to 6
- out_weight: bfloat16 [1024, 2048], P('tp'), may hold values from -0.1875 to 0.1875
- routed_rows: bfloat16 [4096, 2048], P(('ep', 'tp')), may hold values from -6 to 6
- norm_gain: float32 [2048], replicated, may hold values from 0.1 to 1.9
- routing: int32 [4096, 2], P(('ep', 'tp')), may hold values from 0 to 7, all different within a row; in each aligned block of 128 rows (0 to 127, 128 to 255, ...) at most 36 rows name the same one
- route_weight: float32 [4096, 2], P(('ep', 'tp')), may hold values from 0.2 to 1
- gate_weight: bfloat16 [8, 2048, 7168], P('ep', None, 'tp'), may hold values from -0.125 to 0.125
- up_weight: bfloat16 [8, 2048, 7168], P('ep', None, 'tp'), may hold values from -0.125 to 0.125
- down_weight: bfloat16 [8, 7168, 2048], P('ep', 'tp'), may hold values from -0.0625 to 0.0625
Outputs:
- mixed_rows: bfloat16 [8192, 2048], P(('ep', 'tp'))
- expert_mix: bfloat16 [4096, 2048], P(('ep', 'tp'))
Inputs may be any that keep to these rules, and one draw needn't show every extreme that they name: `routing`: each token names 2 different experts. Within the 128 rows of one device no expert is named by more than 36 rows, and in every draw some device's rows name some expert exactly 36 times.
All inputs are finite; a program needn't handle non-finite values.
Results may differ from a plain program's by a relative error of at most 0.012.
Values may be sent and summed in bfloat16 or wider, within the bound.
A program may use at most 128 MiB of HBM per device.

v0:
```python
import jax
import jax.numpy as jnp
from jax import lax
from jax.sharding import PartitionSpec as P

HEAD_DIM = 64
WINDOW = 128
EPS = 1e-06


def padded_2(value, sides, width):
    for axis, dim in sides:
        peers, length = (lax.axis_size(axis), value.shape[dim])
        up = [(i, (i + 1) % peers) for i in range(peers - 1)]
        down = [(j, i) for i, j in up]
        last = lax.slice_in_dim(value, length - width, length, axis=dim)
        leading = lax.slice_in_dim(value, 0, width, axis=dim)
        before = lax.ppermute(last, axis, up)
        after = lax.ppermute(leading, axis, down)
        value = jnp.concatenate([before, value, after], axis=dim)
    return value


def expert_hidden(arrived, gate_weight, up_weight):
    gate_pre = jnp.einsum(
        "scd,df->scf", arrived, gate_weight[0], preferred_element_type=jnp.float32
    )
    up_pre = jnp.einsum("scd,df->scf", arrived, up_weight[0], preferred_element_type=jnp.float32)
    return (jax.nn.silu(gate_pre) * up_pre).astype(jnp.bfloat16)


def window_attention(query_rows, key_rows, value_rows, sink_logit):
    row_count = query_rows.shape[0]
    kv_here = key_rows.shape[1] // HEAD_DIM
    group_size = query_rows.shape[1] // (kv_here * HEAD_DIM)
    block_rows = min(512, row_count)
    joined = jnp.concatenate([key_rows, value_rows], axis=1)
    padded = padded_2(joined, (("ep", 0),), WINDOW)
    seq_total = row_count * lax.axis_size("ep")
    offset = lax.axis_index("ep") * row_count
    sink_col = sink_logit.reshape(kv_here, group_size)[:, :, None]
    score_scale = HEAD_DIM ** (-0.5)

    def one_block(block_index):
        first_row = block_index * block_rows
        query_block = lax.dynamic_slice_in_dim(query_rows, first_row, block_rows, 0).reshape(
            block_rows, kv_here, group_size, HEAD_DIM
        )
        key_span = lax.dynamic_slice_in_dim(padded, first_row, block_rows + 2 * WINDOW, 0)
        key_block = key_span[:, : kv_here * HEAD_DIM].reshape(-1, kv_here, HEAD_DIM)
        value_block = key_span[:, kv_here * HEAD_DIM :].reshape(-1, kv_here, HEAD_DIM)
        scores = (
            jnp.einsum("qkgd,skd->kgqs", query_block, key_block, preferred_element_type=jnp.float32)
            * score_scale
        )
        query_pos = first_row + jnp.arange(block_rows, dtype=jnp.int32)
        key_pos = first_row - WINDOW + jnp.arange(block_rows + 2 * WINDOW, dtype=jnp.int32)
        global_pos = offset + key_pos
        inside = (
            (jnp.abs(key_pos[None, :] - query_pos[:, None]) <= WINDOW)
            & (global_pos >= 0)[None, :]
            & (global_pos < seq_total)[None, :]
        )
        scores = jnp.where(inside, scores, -jnp.inf)
        row_peak = jnp.maximum(jnp.max(scores, axis=-1), sink_col)
        weights = jnp.exp(scores - row_peak[..., None])
        total_weight = jnp.sum(weights, axis=-1) + jnp.exp(sink_col - row_peak)
        attended = jnp.einsum(
            "kgqs,skd->qkgd",
            weights.astype(jnp.bfloat16),
            value_block,
            preferred_element_type=jnp.float32,
        )
        attended = attended / jnp.transpose(total_weight, (2, 0, 1))[..., None]
        return attended.reshape(block_rows, -1).astype(jnp.bfloat16)

    pieces = lax.map(one_block, jnp.arange(row_count // block_rows, dtype=jnp.int32))
    return pieces.reshape(row_count, -1)


def body(
    query_rows,
    key_rows,
    value_rows,
    sink_logit,
    out_weight,
    routed_rows,
    norm_gain,
    routing,
    route_weight,
    gate_weight,
    up_weight,
    down_weight,
):
    attended = window_attention(query_rows, key_rows, value_rows, sink_logit)
    projected = lax.psum_scatter(
        jnp.dot(attended, out_weight, preferred_element_type=jnp.float32).astype(jnp.bfloat16),
        "tp",
        scatter_dimension=0,
        tiled=True,
    )
    token_count, model_width = routed_rows.shape
    top_count = routing.shape[1]
    experts = lax.axis_size("ep")
    capacity = token_count * top_count * 9 // (8 * experts)
    values = routed_rows.astype(jnp.float32)
    normed = (
        values * lax.rsqrt(jnp.mean(values * values, axis=-1, keepdims=True) + EPS) * norm_gain
    ).astype(jnp.bfloat16)
    chosen = routing.reshape(-1)
    onehot = (chosen[:, None] == jnp.arange(experts, dtype=jnp.int32)[None, :]).astype(jnp.int32)
    before = jnp.cumsum(onehot, axis=0) - onehot
    slot_index = jnp.sum(before * onehot, axis=1)
    target = chosen * capacity + slot_index
    outgoing = (
        jnp.zeros((experts * capacity, model_width), jnp.bfloat16)
        .at[target]
        .set(jnp.repeat(normed, top_count, axis=0))
    )
    outgoing = outgoing.reshape(experts, capacity, model_width)
    hidden = expert_hidden(
        lax.all_gather(
            lax.all_to_all(outgoing, "ep", split_axis=0, concat_axis=0, tiled=True),
            "tp",
            axis=0,
            tiled=True,
        ),
        gate_weight,
        up_weight,
    )
    rounded = jnp.einsum(
        "scf,fd->scd", hidden, down_weight[0], preferred_element_type=jnp.float32
    ).astype(jnp.bfloat16)
    summed = lax.psum_scatter(
        lax.optimization_barrier(rounded).astype(jnp.float32).astype(jnp.bfloat16),
        "tp",
        scatter_dimension=0,
        tiled=True,
    ).astype(jnp.float32)
    results = lax.all_to_all(
        summed.astype(jnp.bfloat16), "ep", split_axis=0, concat_axis=0, tiled=True
    ).astype(summed.dtype)
    slot_results = results.reshape(experts * capacity, model_width)
    picked = slot_results[target] * route_weight.reshape(-1)[:, None]
    expert_mix = jnp.sum(picked.reshape(token_count, top_count, model_width), axis=1).astype(
        jnp.bfloat16
    )
    return (projected, expert_mix)


def solution(mesh):
    in_specs = (
        P("ep", "tp"),
        P("ep", "tp"),
        P("ep", "tp"),
        P("tp"),
        P("tp", None),
        P(("ep", "tp"), None),
        P(),
        P(("ep", "tp"), None),
        P(("ep", "tp"), None),
        P("ep", None, "tp"),
        P("ep", None, "tp"),
        P("ep", "tp", None),
    )
    out_specs = (P(("ep", "tp"), None), P(("ep", "tp"), None))
    return jax.shard_map(body, mesh=mesh, in_specs=in_specs, out_specs=out_specs, check_vma=False)
```

profile of v0, /device:TPU:0, one launch (start us, length us, event | category | flops | bytes accessed | tf_op | source)
XLA Modules:
  0.0 254.0 jit_solution(6978425806556693117)
XLA Ops:
  7.2 0.0 copy-start
  7.2 0.0 all-gather.2.cloned.1.call-start
  7.2 0.9 copy.28
  8.1 0.1 eq.29
  8.2 0.1 eq.25
  8.4 0.7 broadcast_multiply_fusion
  9.1 0.6 reduce-window.6
  9.6 0.2 slice_reduce_fusion
  9.9 0.1 copy.27
  10.0 0.1 mul.81
  10.1 1.2 fusion.47
  11.4 1.2 fusion.49
  12.6 0.6 broadcast_in_dim.38
  13.3 1.2 reshape.293
  14.5 0.1 fusion.53
  14.6 3.1 %scatter_custom_fusion = bf16[288,2048]{1,0:T(8,128)(2,1)S(1)} fusion(s32[256]{0:T(256)S(1)} %bitcast.135, bf16[256,2048]{1,0:T(8,128)(2,1)} %reshape.293, bf16[]{:T(256)} %constant.85.clone.1), kind=kCustom, calls=%fused_computation.52 | custom fusion | bytes 1180160 | tf_op jit(solution)/shard_map/scatter | solution.py:118
  17.7 0.3 reshape.276
  18.0 38.5 %all_to_all.10 = bf16[8,36,2048]{2,1,0:T(8,128)(2,1)S(1)} all-to-all(bf16[8,36,2048]{2,1,0:T(8,128)(2,1)S(1)} %reshape.276), channel_id=1, replica_groups=mesh['ep'=8,'tp'=4] {'ep'}, dimensions={0} | all-to-all | bytes 2359296 | tf_op jit(solution)/shard_map/all_to_all | solution.py:123
  56.5 1.7 copy.30
  58.2 0.0 all-gather.2.cloned.1.call-update
  58.2 0.0 reduce-scatter.5.cloned.1.call-start
  58.2 36.5 %all-gather.2.cloned.1.call-done = bf16[32,36,2048]{2,0,1:T(8,128)(2,1)} async-done(((bf16[8,36,2048]{2,0,1:T(8,128)(2,1)}), bf16[32,36,2048]{2,0,1:T(8,128)(2,1)}) %all-gather.2.cloned.1.call-update) | async-done | bytes 4718608 | tf_op jit(solution)/shard_map/all_gather | solution.py:122
  94.8 19.5 %fusion.28 = f32[32,36,1792]{2,1,0:T(8,128)} fusion(bf16[1,2048,1792]{2,1,0:T(8,128)(2,1)} %param.24, bf16[32,36,2048]{2,0,1:T(8,128)(2,1)} %all-gather.2.cloned.1.call-done), kind=kOutput, calls=%fused_computation.37 | convolution fusion | flops 8455716864 | bytes 20316160 | tf_op jit(solution)/shard_map/scd,df->scf/dot_general | solution.py:28
  114.3 33.8 %fusion.40 = bf16[32,36,2048]{2,1,0:T(8,128)(2,1)} fusion(bf16[1,1792,2048]{2,1,0:T(8,128)(2,1)} %param.25, f32[32,36,1792]{2,1,0:T(8,128)} %fusion.28, bf16[1,2048,1792]{2,1,0:T(8,128)(2,1)} %param.23, bf16[32,36,2048]{2,0,1:T(8,128)(2,1)} %all-gather.2.cloned.1.call-done), kind=kOutput, calls=%fused_computation.44 | convolution fusion | flops 16926179328 | bytes 32374784 | tf_op jit(solution)/shard_map/scf,fd->scd/dot_general | solution.py:131
  148.1 0.0 reduce-scatter.5.cloned.1.call-update
  148.1 0.0 reduce-scatter.3.cloned.1.call-start
  148.2 0.0 copy-done.3
  148.2 3.5 %collective-permute-start = (bf16[128,128]{0,1:T(8,128)(2,1)S(1)}, bf16[128,128]{0,1:T(8,128)(2,1)S(1)}, u32[]{:S(2)}, u32[]{:S(2)}) collective-permute-start(bf16[128,128]{0,1:T(8,128)(2,1)S(1)} %get-tuple-element.131), channel_id=1, source_target_pairs={{0,4},{4,8},{8,12},{12,16},{16,20},{20,24},{24,28},{1,5},{5,9},{9,... | collective-permute-start | bytes 98312 | tf_op jit(solution)/shard_map/ppermute | solution.py:18
  151.8 1.3 collective-permute-start.1
  153.1 0.3 collective-permute-done
  153.3 4.2 %collective-permute-done.1 = bf16[128,128]{0,1:T(8,128)(2,1)S(1)} collective-permute-done((bf16[128,128]{0,1:T(8,128)(2,1)S(1)}, bf16[128,128]{0,1:T(8,128)(2,1)S(1)}, u32[]{:S(2)}, u32[]{:S(2)}) %collective-permute-start.1) | collective-permute-done | bytes 32800 | tf_op jit(solution)/shard_map/ppermute | solution.py:19
  157.6 25.5 %while.12 = (s32[]{:T(128)}, bf16[2,512,256]{2,1,0:T(8,128)(2,1)S(1)}, s32[2]{0:T(128)S(1)}, bf16[1280,128]{0,1:T(8,128)(2,1)S(1)}, s32[]{:T(128)}, /*index=5*/b...) while((s32[]{:T(128)}, ...), condition=%wide.region_3.4_spmd, body=%wide.region_0.3_spmd.sunk | while | flops 422191360 | bytes 48526672 | solution.py:77
  157.9 0.7 dynamic_slice.23
  159.2 0.8 fusion.69
  160.1 0.1 copy.47
  160.2 1.2 fusion.70
  161.4 0.1 broadcast_maximum_fusion.2
  161.5 2.6 %copy-done.1 = f32[768,512,4]{1,0,2:T(8,128)} copy-done((f32[768,512,4]{1,0,2:T(8,128)}, f32[768,512,4]{1,0,2:T(8,128)S(1)}, u32[]{:S(2)}) %copy-start.1) | copy-done | bytes 6291480 | tf_op jit(solution)/shard_map/while
  164.1 1.4 fusion.71
  165.5 0.1 fusion.72
  165.5 5.0 %fusion.73 = bf16[512,1,4,64]{0,3,2,1:T(8,128)(2,1)S(1)} fusion(f32[768,512,4]{1,0,2:T(8,128)} %copy-done.1, f32[4,512]{1,0:T(4,128)S(1)} %broadcast_maximum_fusion.2, pred[512,768]{0,1:T(8,128)(4,1)S(1)} %fusion.69, f32[512,4]{0,1:T(4,128)S(1)} %fusion.72, bf16[1280,128]{0,1:T(8,128)(2,1)S(1)} %get-tuple-element.215, s32[]{:T(128)S(6)} %select_n.57, ...), kind=kOutput, calls=%fused_computation.15.clone.1 | convolution fusion | flops 207880192 | bytes 7061512 | tf_op jit(solution)/shard_map/while/body/eval_jaxpr/kgqs,skd->qkgd/dot_general | solution.py:68
  170.5 0.1 copy.48
  170.7 0.7 dynamic_slice.23
  172.1 0.8 fusion.69
  172.9 0.1 copy.47
  173.1 1.2 fusion.70
  174.3 0.1 broadcast_maximum_fusion.2
  174.4 2.6 %copy-done.1 = f32[768,512,4]{1,0,2:T(8,128)} copy-done((f32[768,512,4]{1,0,2:T(8,128)}, f32[768,512,4]{1,0,2:T(8,128)S(1)}, u32[]{:S(2)}) %copy-start.1) | copy-done | bytes 6291480 | tf_op jit(solution)/shard_map/while
  176.9 1.4 fusion.71
  178.3 0.1 fusion.72
  178.4 4.6 %fusion.73 = bf16[512,1,4,64]{0,3,2,1:T(8,128)(2,1)S(1)} fusion(f32[768,512,4]{1,0,2:T(8,128)} %copy-done.1, f32[4,512]{1,0:T(4,128)S(1)} %broadcast_maximum_fusion.2, pred[512,768]{0,1:T(8,128)(4,1)S(1)} %fusion.69, f32[512,4]{0,1:T(4,128)S(1)} %fusion.72, bf16[1280,128]{0,1:T(8,128)(2,1)S(1)} %get-tuple-element.215, s32[]{:T(128)S(6)} %select_n.57, ...), kind=kOutput, calls=%fused_computation.15.clone.1 | convolution fusion | flops 207880192 | bytes 7061512 | tf_op jit(solution)/shard_map/while/body/eval_jaxpr/kgqs,skd->qkgd/dot_general | solution.py:68
  182.9 0.1 copy.48
  183.1 0.0 copy-start.6
  183.2 3.2 %convolution_convert_fusion = bf16[1024,2048]{1,0:T(8,128)(2,1)} fusion(bf16[1024,256]{1,0:T(8,128)(2,1)S(1)} %bitcast.131, bf16[256,2048]{1,0:T(8,128)(2,1)S(1)} %copy-done), kind=kOutput, calls=%fused_computation.45 | convolution fusion | flops 1075838976 | bytes 5767168 | tf_op jit(solution)/shard_map/dot_general | solution.py:97
  186.3 0.0 reduce-scatter.3.cloned.1.call-update
  186.4 13.3 %reduce-scatter.5.cloned.1.call-done = bf16[8,36,2048]{2,1,0:T(8,128)(2,1)} async-done(((bf16[32,36,2048]{2,1,0:T(8,128)(2,1)}), bf16[8,36,2048]{2,1,0:T(8,128)(2,1)}) %reduce-scatter.5.cloned.1.call-update) | async-done | bytes 1179664 | tf_op jit(solution)/shard_map/reduce_scatter | solution.py:134
  199.6 5.5 %all-to-all-start.1 = ((bf16[8,36,2048]{2,1,0:T(8,128)(2,1)}), bf16[8,36,2048]{2,1,0:T(8,128)(2,1)}, u32[]{:S(2)}, u32[]{:S(2)}) async-start(bf16[8,36,2048]{2,1,0:T(8,128)(2,1)} %reduce-scatter.5.cloned.1.call-done), calls=%async_computation.3 | async-start | bytes 2621440 | tf_op jit(solution)/shard_map/all_to_all | solution.py:140
  205.2 0.1 copy.33
  205.3 31.2 %all-to-all-done.1 = bf16[8,36,2048]{2,1,0:T(8,128)(2,1)} async-done(((bf16[8,36,2048]{2,1,0:T(8,128)(2,1)}), bf16[8,36,2048]{2,1,0:T(8,128)(2,1)}, u32[]{:S(2)}, u32[]{:S(2)}) %all-to-all-start.1) | async-done | bytes 1179680 | tf_op jit(solution)/shard_map/all_to_all | solution.py:140
  236.5 1.4 reshape.280
  237.9 2.7 %gather_fusion = f32[256,2048]{1,0:T(8,128)} fusion(f32[288,2048]{1,0:T(8,128)S(1)} %reshape.280, s32[1024]{0:T(1024)S(1)} %pad_clamp_fusion), kind=kCustom, calls=%fused_computation | custom fusion | bytes 4195328 | tf_op jit(solution)/shard_map/gather | solution.py:144
  240.6 2.5 gather.6
  243.1 3.9 %multiply_reduce_fusion = bf16[128,2048]{1,0:T(8,128)(2,1)} fusion(f32[128,2,2048]{2,1,0:T(2,128)S(1)} %gather.6, f32[128,2]{1,0:T(8,128)S(1)} %copy.33), kind=kLoop, calls=%fused_computation.46 | loop fusion | flops 786432 | bytes 2622464 | tf_op jit(solution)/shard_map/reduce_sum | solution.py:145
  247.0 0.4 reduce-scatter.3.cloned.1.call-done
  (33 shorter events, 0.3 us)
Async XLA Ops:
  7.2 176.0 %copy-start = (bf16[256,2048]{1,0:T(8,128)(2,1)S(1)}, bf16[256,2048]{1,0:T(8,128)(2,1)}, u32[]{:S(2)}) copy-start(bf16[256,2048]{1,0:T(8,128)(2,1)} %param.18) | copy-start | bytes 3145732
  7.2 87.6 %all-gather.2.cloned.1.call-start = ((), (), s32[]{:S(2)}) async-start(), calls=%async_computation.5 | async-start | bytes 5898240 | tf_op jit(solution)/shard_map/all_gather | solution.py:122
  58.2 141.4 %reduce-scatter.5.cloned.1.call-start = ((), (), s32[]{:S(2)}) async-start(), calls=%async_computation.6 | async-start | bytes 6553600 | tf_op jit(solution)/shard_map/reduce_scatter | solution.py:134
  114.3 33.9 %copy-start.3 = (bf16[1024,64]{0,1:T(8,128)(2,1)S(1)}, bf16[1024,64]{0,1:T(8,128)(2,1)}, u32[]{:S(2)}) copy-start(bf16[1024,64]{0,1:T(8,128)(2,1)} %param.15) | copy-start | bytes 393220
  114.3 33.9 %copy-start.4 = (bf16[1024,64]{0,1:T(8,128)(2,1)S(1)}, bf16[1024,64]{0,1:T(8,128)(2,1)}, u32[]{:S(2)}) copy-start(bf16[1024,64]{0,1:T(8,128)(2,1)} %param.16) | copy-start | bytes 393220
  148.1 9.5 %copy-start.2 = (bf16[1024,256]{1,0:T(8,128)(2,1)S(1)}, bf16[1024,256]{1,0:T(8,128)(2,1)}, u32[]{:S(2)}) copy-start(bf16[1024,256]{1,0:T(8,128)(2,1)} %param.14) | copy-start | bytes 1572868
  148.1 9.5 %copy-start.5 = (f32[4]{0:T(128)S(1)}, f32[4]{0:T(128)}, u32[]{:S(2)}) copy-start(f32[4]{0:T(128)} %param.17) | copy-start | bytes 52
  148.1 99.3 %reduce-scatter.3.cloned.1.call-start = ((), (), s32[]{:S(2)}) async-start(), calls=%async_computation.4 | async-start | bytes 5242880 | tf_op jit(solution)/shard_map/reduce_scatter | solution.py:96
  148.2 5.1 %collective-permute-start = (bf16[128,128]{0,1:T(8,128)(2,1)S(1)}, bf16[128,128]{0,1:T(8,128)(2,1)S(1)}, u32[]{:S(2)}, u32[]{:S(2)}) collective-permute-start(bf16[128,128]{0,1:T(8,128)(2,1)S(1)} %get-tuple-element.131), channel_id=1, source_target_pairs={{0,4},{4,8},{8,12},{12,16},{16,20},{20,24},{24,28},{1,5},{5,9},{9,... | collective-permute-start | bytes 98312 | tf_op jit(solution)/shard_map/ppermute | solution.py:18
  151.8 5.8 %collective-permute-start.1 = (bf16[128,128]{0,1:T(8,128)(2,1)S(1)}, bf16[128,128]{0,1:T(8,128)(2,1)S(1)}, u32[]{:S(2)}, u32[]{:S(2)}) collective-permute-start(bf16[128,128]{0,1:T(8,128)(2,1)S(1)} %get-tuple-element.132), channel_id=1, source_target_pairs={{4,0},{8,4},{12,8},{16,12},{20,16},{24,20},{28,24},{5,1},{9,5},{13... | collective-permute-start | bytes 98312 | tf_op jit(solution)/shard_map/ppermute | solution.py:19
  161.4 2.7 %copy-start.1 = (f32[768,512,4]{1,0,2:T(8,128)}, f32[768,512,4]{1,0,2:T(8,128)S(1)}, u32[]{:S(2)}) copy-start(f32[768,512,4]{1,0,2:T(8,128)S(1)} %get-tuple-element.182) | copy-start | bytes 18874372 | tf_op jit(solution)/shard_map/while
  174.3 2.7 %copy-start.1 = (f32[768,512,4]{1,0,2:T(8,128)}, f32[768,512,4]{1,0,2:T(8,128)S(1)}, u32[]{:S(2)}) copy-start(f32[768,512,4]{1,0,2:T(8,128)S(1)} %get-tuple-element.182) | copy-start | bytes 18874372 | tf_op jit(solution)/shard_map/while
  183.1 22.0 %copy-start.6 = (f32[128,2]{0,1:T(2,128)S(1)}, f32[128,2]{0,1:T(2,128)}, u32[]{:S(2)}) copy-start(f32[128,2]{0,1:T(2,128)} %param.22) | copy-start | bytes 3076
  199.6 36.8 %all-to-all-start.1 = ((bf16[8,36,2048]{2,1,0:T(8,128)(2,1)}), bf16[8,36,2048]{2,1,0:T(8,128)(2,1)}, u32[]{:S(2)}, u32[]{:S(2)}) async-start(bf16[8,36,2048]{2,1,0:T(8,128)(2,1)} %reduce-scatter.5.cloned.1.call-done), calls=%async_computation.3 | async-start | bytes 2621440 | tf_op jit(solution)/shard_map/all_to_all | solution.py:140
Sparse Core Ops, SparseCore 0:
  58.3 36.4 all-gather.1
  148.2 51.3 reduce-scatter.4
  202.7 44.6 reduce-scatter.2
where the time goes:
time: 254 us
  waiting for transfers between devices  86 us (34%)
  matrix products  68.4 us (27%)
  blocking collectives  38.5 us (15%)
  local copies, waits for them, and re-layouts  22.4 us (9%)
  between operations  13.9 us (5%)
  other arithmetic  12.5 us (5%)
  starting transfers between devices  10.4 us (4%)
    all_to_all x1, blocking collectives, body(): lax.all_to_all(outgoing, 'ep', split_axis=0, concat_axis=0, tiled=True)  38.5 us
    all_gather x1, waiting for transfers between devices, body(): lax.all_gather(lax.all_to_all(outgoing, 'ep', split_axis=0, concat_axis=0...  36.5 us
    dot_general x1, matrix products, body(): jnp.einsum('scf,fd->scd', hidden, down_weight[0], preferred_element_type=...  33.8 us
    all_to_all x1, waiting for transfers between devices, body(): lax.all_to_all(summed.astype(jnp.bfloat16), 'ep', split_axis=0, concat_ax...  31.2 us
    dot_general x1, matrix products, expert_hidden(): jnp.einsum('scd,df->scf', arrived, up_weight[0], preferred_element_type=j...  19.5 us
    reduce_scatter x1, waiting for transfers between devices, body(): lax.psum_scatter(lax.optimization_barrier(rounded).astype(jnp.float32).as...  13.3 us
    dot_general x2, matrix products, one_block(): jnp.einsum('kgqs,skd->qkgd', weights.astype(jnp.bfloat16), value_block, p...  9.53 us
    all_to_all x1, starting transfers between devices, body(): lax.all_to_all(summed.astype(jnp.bfloat16), 'ep', split_axis=0, concat_ax...  5.52 us
  transfers between devices with their start and end apart: 6, of which 6 were waited for; matrix products, arithmetic and copies ran while one was open for 13% of the time, Pallas kernels for 0%

commit v1 on v0

--- a/solution.py
+++ b/solution.py
@@ -1,3 +1,4 @@
+import functools
 import jax
 import jax.numpy as jnp
 from jax import lax
@@ -6,6 +7,31 @@
 HEAD_DIM = 64
 WINDOW = 128
 EPS = 1e-06
+
+
+def trace_heaps(row_data, shard_axis):
+    n_peers_all = lax.psum(1, shard_axis)
+    all_rows = []
+    for s in range(n_peers_all):
+        all_rows.append((s, (s + 1) % n_peers_all))
+    samples = []
+    for s in range(n_peers_all):
+        samples.append((s, (s - 1) % n_peers_all))
+    parts_out, even = ([row_data], [row_data])
+    for _ in range(n_peers_all // 2):
+        g_now = lax.ppermute(parts_out[-1], shard_axis, all_rows)
+        parts_out.append(g_now)
+    for _ in range((n_peers_all - 1) // 2):
+        v1 = lax.ppermute(even[-1], shard_axis, samples)
+        even.append(v1)
+    b_next = jnp.concatenate([*parts_out[::-1], *even[1:]], 0)
+    next_value = jnp.roll(
+        b_next, (lax.axis_index(shard_axis) - n_peers_all // 2) * row_data.shape[0], 0
+    )
+    return next_value
+
+
+link_the_screen = functools.partial(trace_heaps, shard_axis="tp")
 
 
 def padded_2(value, sides, width):
@@ -119,12 +145,7 @@
     )
     outgoing = outgoing.reshape(experts, capacity, model_width)
     hidden = expert_hidden(
-        lax.all_gather(
-            lax.all_to_all(outgoing, "ep", split_axis=0, concat_axis=0, tiled=True),
-            "tp",
-            axis=0,
-            tiled=True,
-        ),
+        link_the_screen(lax.all_to_all(outgoing, "ep", split_axis=0, concat_axis=0, tiled=True)),
         gate_weight,
         up_weight,
     )

time: 254 us -> 259 us (1.020)
  matrix products: 68.4 us -> 58 us
  local copies, waits for them, and re-layouts: 22.4 us -> 32 us
  waiting for transfers between devices: 86 us -> 89.5 us
    ppermute x0 -> x3, waiting for transfers between devices: none -> 40.2 us  [the longest x2 40.2 us: trace_heaps(): g_now = lax.ppermute(parts_out[-1], shard_axis, all_rows)]
    all_gather x1 -> x0, waiting for transfers between devices: 36.5 us -> none  [body(): lax.all_gather(lax.all_to_all(outgoing, 'ep', split_axis=0, concat_axis=0...]
    unnamed x15 -> x30, local copies, waits for them, and re-layouts: 1.02 us -> 11.4 us
    dot_general x1, matrix products: 19.5 us -> 12 us  [expert_hidden(): jnp.einsum('scd,df->scf', arrived, gate_weight[0], preferred_element_type...]
    dot_general x1, matrix products: 33.8 us -> 30.8 us  [body(): jnp.einsum('scf,fd->scd', hidden, down_weight[0], preferred_element_type=...]
  transfers between devices with their start and end apart: 6 -> 8, of which waited for: 6 -> 7; matrix products, arithmetic and copies ran while one was open for 13% -> 14% of each run, Pallas kernels for 0% -> 0%
where the time goes in v1:
time: 259 us
  waiting for transfers between devices  89.5 us (35%)
  matrix products  58 us (22%)
  blocking collectives  38.7 us (15%)
  local copies, waits for them, and re-layouts  32 us (12%)
  between operations  14.3 us (6%)
  other arithmetic  12.5 us (5%)
  starting transfers between devices  12.1 us (5%)
    ppermute x2, waiting for transfers between devices, trace_heaps(): g_now = lax.ppermute(parts_out[-1], shard_axis, all_rows)  40.2 us
    all_to_all x1, blocking collectives, body(): lax.all_to_all(outgoing, 'ep', split_axis=0, concat_axis=0, tiled=True)  38.7 us
    all_to_all x1, waiting for transfers between devices, body(): lax.all_to_all(summed.astype(jnp.bfloat16), 'ep', split_axis=0, concat_ax...  31.2 us
    dot_general x1, matrix products, body(): jnp.einsum('scf,fd->scd', hidden, down_weight[0], preferred_element_type=...  30.8 us
    reduce_scatter x1, waiting for transfers between devices, body(): lax.psum_scatter(lax.optimization_barrier(rounded).astype(jnp.float32).as...  13.2 us
    dot_general x1, matrix products, expert_hidden(): jnp.einsum('scd,df->scf', arrived, gate_weight[0], preferred_element_type...  12 us
    unnamed x30, local copies, waits for them, and re-layouts  11.4 us
    dot_general x2, matrix products, one_block(): jnp.einsum('kgqs,skd->qkgd', weights.astype(jnp.bfloat16), value_block, p...  9.55 us
  transfers between devices with their start and end apart: 8, of which 7 were waited for; matrix products, arithmetic and copies ran while one was open for 14% of the time, Pallas kernels for 0%

profile of v1, /device:TPU:0, one launch (start us, length us, event | category | flops | bytes accessed | tf_op | source)
XLA Modules:
  0.0 258.9 jit_solution(16411483189059662616)
XLA Ops:
  7.2 0.9 copy.28
  8.1 0.1 eq.32
  8.2 0.1 eq.28
  8.4 0.7 broadcast_multiply_fusion
  9.1 0.6 reduce-window.6
  9.6 0.2 slice_reduce_fusion
  9.9 0.1 copy.27
  10.0 0.1 mul.84
  10.1 1.2 fusion.47
  11.4 1.2 fusion.49
  12.6 0.6 broadcast_in_dim.38
  13.3 0.4 reshape.293
  13.7 0.1 fusion.53
  13.8 2.5 scatter_custom_fusion
  16.3 1.2 reshape.276
  17.5 38.7 %all_to_all.10 = bf16[8,36,2048]{2,1,0:T(8,128)(2,1)S(1)} all-to-all(bf16[8,36,2048]{2,1,0:T(8,128)(2,1)} %reshape.276), channel_id=1, replica_groups=mesh['ep'=8,'tp'=4] {'ep'}, dimensions={0} | all-to-all | bytes 2359296 | tf_op jit(solution)/shard_map/all_to_all | solution.py:148
  56.2 0.7 copy.30
  56.9 15.6 %collective-permute-done.2 = bf16[8,36,2048]{2,0,1:T(8,128)(2,1)S(1)} collective-permute-done((bf16[8,36,2048]{2,0,1:T(8,128)(2,1)S(1)}, bf16[8,36,2048]{2,0,1:T(8,128)(2,1)S(1)}, u32[]{:S(2)}, u32[]{:S(2)}) %collective-permute-start.2) | collective-permute-done | bytes 1179680 | tf_op jit(solution)/shard_map/ppermute | solution.py:22
  72.5 1.7 collective-permute-start.4
  74.3 24.6 %collective-permute-done.3 = bf16[8,36,2048]{2,0,1:T(8,128)(2,1)} collective-permute-done((bf16[8,36,2048]{2,0,1:T(8,128)(2,1)S(1)}, bf16[8,36,2048]{2,0,1:T(8,128)(2,1)}, u32[]{:S(2)}, u32[]{:S(2)}) %collective-permute-start.3) | collective-permute-done | bytes 1179680 | tf_op jit(solution)/shard_map/ppermute | solution.py:22
  98.9 1.9 copy_dynamic-update-slice_fusion.4
  100.8 0.7 copy_dynamic-update-slice_fusion.2
  101.5 0.1 constant_dynamic-update-slice_fusion.4
  101.6 0.7 copy_dynamic-update-slice_fusion
  102.3 2.3 copy_dynamic-update-slice_fusion.5
  104.6 0.7 copy_dynamic-update-slice_fusion.3
  105.3 0.1 constant_dynamic-update-slice_fusion.3
  105.4 0.7 copy_dynamic-update-slice_fusion.1
  106.0 4.0 %copy-done.2 = bf16[64,36,2048]{2,1,0:T(8,128)(2,1)} copy-done((bf16[64,36,2048]{2,1,0:T(8,128)(2,1)}, bf16[64,36,2048]{2,1,0:T(8,128)(2,1)S(1)}, u32[]{:S(2)}) %copy-start.2) | copy-done | bytes 9437208
  110.0 12.0 %fusion.30 = f32[32,36,1792]{2,1,0:T(8,128)} fusion(bf16[1,2048,1792]{2,1,0:T(8,128)(2,1)S(1)} %bitcast.139, bf16[64,36,2048]{2,1,0:T(8,128)(2,1)S(1)} %copy_dynamic-update-slice_fusion.1, s32[]{:T(128)S(6)} %select_n.45), kind=kOutput, calls=%fused_computation.39 | convolution fusion | flops 8455716864 | bytes 20840452 | tf_op jit(solution)/shard_map/scd,df->scf/dot_general | solution.py:51
  122.1 30.8 %fusion.40 = bf16[32,36,2048]{2,1,0:T(8,128)(2,1)} fusion(bf16[1,1792,2048]{2,1,0:T(8,128)(2,1)} %param.25, f32[32,36,1792]{2,1,0:T(8,128)} %fusion.30, bf16[1,2048,1792]{2,1,0:T(8,128)(2,1)} %param.24, bf16[64,36,2048]{2,1,0:T(8,128)(2,1)} %copy-done.2, s32[]{:T(128)S(6)} %select_n.45), kind=kOutput, calls=%fused_computation.44 | convolution fusion | flops 16926179328 | bytes 33816580 | tf_op jit(solution)/shard_map/scf,fd->scd/dot_general | solution.py:152
  153.0 3.5 %collective-permute-start = (bf16[128,128]{0,1:T(8,128)(2,1)S(1)}, bf16[128,128]{0,1:T(8,128)(2,1)S(1)}, u32[]{:S(2)}, u32[]{:S(2)}) collective-permute-start(bf16[128,128]{0,1:T(8,128)(2,1)S(1)} %get-tuple-element.131), channel_id=1, source_target_pairs={{0,4},{4,8},{8,12},{12,16},{16,20},{20,24},{24,28},{1,5},{5,9},{9,... | collective-permute-start | bytes 98312 | tf_op jit(solution)/shard_map/ppermute | solution.py:44
  156.5 1.3 collective-permute-start.1
  157.8 0.3 collective-permute-done
  158.1 4.2 %collective-permute-done.1 = bf16[128,128]{0,1:T(8,128)(2,1)S(1)} collective-permute-done((bf16[128,128]{0,1:T(8,128)(2,1)S(1)}, bf16[128,128]{0,1:T(8,128)(2,1)S(1)}, u32[]{:S(2)}, u32[]{:S(2)}) %collective-permute-start.1) | collective-permute-done | bytes 32800 | tf_op jit(solution)/shard_map/ppermute | solution.py:45
  162.4 25.6 %while.12 = (s32[]{:T(128)}, bf16[2,512,256]{2,1,0:T(8,128)(2,1)S(1)}, s32[2]{0:T(128)S(1)}, bf16[1280,128]{0,1:T(8,128)(2,1)S(1)}, s32[]{:T(128)}, /*index=5*/b...) while((s32[]{:T(128)}, ...), condition=%wide.region_3.4_spmd, body=%wide.region_0.3_spmd.sunk | while | flops 422191360 | bytes 48526672 | solution.py:103
  162.6 0.7 dynamic_slice.35
  164.0 0.8 fusion.72
  164.8 0.1 copy.51
  165.0 1.2 fusion.73
  166.3 2.6 copy-done.1
  168.9 1.4 fusion.74
  170.2 0.1 fusion.75
  170.3 5.0 %fusion.76 = bf16[512,1,4,64]{0,3,2,1:T(8,128)(2,1)S(1)} fusion(f32[768,512,4]{1,0,2:T(8,128)} %copy-done.1, f32[4,512]{1,0:T(4,128)S(1)} %broadcast_maximum_fusion.2, pred[512,768]{0,1:T(8,128)(4,1)S(1)} %fusion.72, f32[512,4]{0,1:T(4,128)S(1)} %fusion.75, bf16[1280,128]{0,1:T(8,128)(2,1)S(1)} %get-tuple-element.215, s32[]{:T(128)S(6)} %select_n.72, ...), kind=kOutput, calls=%fused_computation.15.clone.1 | convolution fusion | flops 207880192 | bytes 7061512 | tf_op jit(solution)/shard_map/while/body/eval_jaxpr/kgqs,skd->qkgd/dot_general | solution.py:94
  175.3 0.1 copy.52
  175.5 0.7 dynamic_slice.35
  176.9 0.8 fusion.72
  177.7 0.1 copy.51
  177.9 1.2 fusion.73
  179.2 2.6 copy-done.1
  181.7 1.4 fusion.74
  183.1 0.1 fusion.75
  183.2 4.6 %fusion.76 = bf16[512,1,4,64]{0,3,2,1:T(8,128)(2,1)S(1)} fusion(f32[768,512,4]{1,0,2:T(8,128)} %copy-done.1, f32[4,512]{1,0:T(4,128)S(1)} %broadcast_maximum_fusion.2, pred[512,768]{0,1:T(8,128)(4,1)S(1)} %fusion.72, f32[512,4]{0,1:T(4,128)S(1)} %fusion.75, bf16[1280,128]{0,1:T(8,128)(2,1)S(1)} %get-tuple-element.215, s32[]{:T(128)S(6)} %select_n.72, ...), kind=kOutput, calls=%fused_computation.15.clone.1 | convolution fusion | flops 207880192 | bytes 7061512 | tf_op jit(solution)/shard_map/while/body/eval_jaxpr/kgqs,skd->qkgd/dot_general | solution.py:94
  187.7 0.1 copy.52
  188.0 3.2 %convolution_convert_fusion = bf16[1024,2048]{1,0:T(8,128)(2,1)} fusion(bf16[1024,256]{1,0:T(8,128)(2,1)S(1)} %bitcast.131, bf16[256,2048]{1,0:T(8,128)(2,1)S(1)} %copy-done), kind=kOutput, calls=%fused_computation.45 | convolution fusion | flops 1075838976 | bytes 5767168 | tf_op jit(solution)/shard_map/dot_general | solution.py:123
  191.2 13.2 %reduce-scatter.5.cloned.1.call-done = bf16[8,36,2048]{2,1,0:T(8,128)(2,1)} async-done(((bf16[32,36,2048]{2,1,0:T(8,128)(2,1)}), bf16[8,36,2048]{2,1,0:T(8,128)(2,1)}) %reduce-scatter.5.cloned.1.call-update) | async-done | bytes 1179664 | tf_op jit(solution)/shard_map/reduce_scatter | solution.py:155
  204.4 5.5 %all-to-all-start.1 = ((bf16[8,36,2048]{2,1,0:T(8,128)(2,1)}), bf16[8,36,2048]{2,1,0:T(8,128)(2,1)}, u32[]{:S(2)}, u32[]{:S(2)}) async-start(bf16[8,36,2048]{2,1,0:T(8,128)(2,1)} %reduce-scatter.5.cloned.1.call-done), calls=%async_computation.3 | async-start | bytes 2621440 | tf_op jit(solution)/shard_map/all_to_all | solution.py:161
  209.9 0.1 copy.38
  210.0 31.2 %all-to-all-done.1 = bf16[8,36,2048]{2,1,0:T(8,128)(2,1)} async-done(((bf16[8,36,2048]{2,1,0:T(8,128)(2,1)}), bf16[8,36,2048]{2,1,0:T(8,128)(2,1)}, u32[]{:S(2)}, u32[]{:S(2)}) %all-to-all-start.1) | async-done | bytes 1179680 | tf_op jit(solution)/shard_map/all_to_all | solution.py:161
  241.2 1.4 reshape.280
  242.6 2.7 %gather_fusion = f32[256,2048]{1,0:T(8,128)} fusion(f32[288,2048]{1,0:T(8,128)S(1)} %reshape.280, s32[1024]{0:T(1024)S(1)} %pad_clamp_fusion), kind=kCustom, calls=%fused_computation | custom fusion | bytes 4195328 | tf_op jit(solution)/shard_map/gather | solution.py:165
  245.3 2.5 gather.6
  247.8 3.9 %multiply_reduce_fusion = bf16[128,2048]{1,0:T(8,128)(2,1)} fusion(f32[128,2,2048]{2,1,0:T(2,128)S(1)} %gather.6, f32[128,2]{1,0:T(8,128)S(1)} %copy.38), kind=kLoop, calls=%fused_computation.46 | loop fusion | flops 786432 | bytes 2622464 | tf_op jit(solution)/shard_map/reduce_sum | solution.py:166
  251.7 0.3 reduce-scatter.3.cloned.1.call-done
  (53 shorter events, 0.7 us)
Async XLA Ops:
  7.2 180.8 %copy-start = (bf16[256,2048]{1,0:T(8,128)(2,1)S(1)}, bf16[256,2048]{1,0:T(8,128)(2,1)}, u32[]{:S(2)}) copy-start(bf16[256,2048]{1,0:T(8,128)(2,1)} %param.18) | copy-start | bytes 3145732
  7.2 197.2 %reduce-scatter.5.cloned.1.call-start = ((), (), s32[]{:S(2)}) async-start(), calls=%async_computation.5 | async-start | bytes 6553600 | tf_op jit(solution)/shard_map/reduce_scatter | solution.py:155
  56.8 15.7 %copy-start.4 = (bf16[8,36,2048]{2,0,1:T(8,128)(2,1)}, bf16[8,36,2048]{2,0,1:T(8,128)(2,1)S(1)}, u32[]{:S(2)}) copy-start(bf16[8,36,2048]{2,0,1:T(8,128)(2,1)S(1)} %copy.30) | copy-start | bytes 3538948
  56.8 15.7 %collective-permute-start.2 = (bf16[8,36,2048]{2,0,1:T(8,128)(2,1)S(1)}, bf16[8,36,2048]{2,0,1:T(8,128)(2,1)S(1)}, u32[]{:S(2)}, u32[]{:S(2)}) collective-permute-start(bf16[8,36,2048]{2,0,1:T(8,128)(2,1)S(1)} %copy.30), channel_id=1, source_target_pairs={{0,1},{1,2},{2,3},{3,0},{4,5},{5,6},{6,7},{7,4},{8,9},{9,10},{10,1... | collective-permute-start | bytes 3538952 | tf_op jit(solution)/shard_map/ppermute | solution.py:22
  72.5 26.4 %collective-permute-start.3 = (bf16[8,36,2048]{2,0,1:T(8,128)(2,1)S(1)}, bf16[8,36,2048]{2,0,1:T(8,128)(2,1)}, u32[]{:S(2)}, u32[]{:S(2)}) collective-permute-start(bf16[8,36,2048]{2,0,1:T(8,128)(2,1)S(1)} %collective-permute-done.2), channel_id=1, source_target_pairs={{0,1},{1,2},{2,3},{3,0},{4,5},{5,6},{6,7},{7,4},{8,9},{9,10},{10,1... | collective-permute-start | bytes 3538952 | tf_op jit(solution)/shard_map/ppermute | solution.py:22
  72.5 29.1 %collective-permute-start.4 = (bf16[8,36,2048]{2,0,1:T(8,128)(2,1)}, bf16[8,36,2048]{2,0,1:T(8,128)(2,1)S(1)}, u32[]{:S(2)}, u32[]{:S(2)}) collective-permute-start(bf16[8,36,2048]{2,0,1:T(8,128)(2,1)} %copy-done.4), channel_id=1, source_target_pairs={{0,3},{1,0},{2,1},{3,2},{4,7},{5,4},{6,5},{7,6},{8,11},{9,8},{10,9... | collective-permute-start | bytes 3538952 | tf_op jit(solution)/shard_map/ppermute | solution.py:25
  101.5 8.5 %slice-start = ((s8[7340032]{0:T(1024)(128)(4,1)}), s8[4194304]{0:T(1024)(128)(4,1)S(1)}, s32[]{:S(2)}) async-start(s8[7340032]{0:T(1024)(128)(4,1)} %bitcast.138), calls=%async_computation.6 | async-start | bytes 8388608
  102.3 7.8 %slice-start.1 = ((s8[7340032]{0:T(1024)(128)(4,1)}), s8[3145728]{0:T(1024)(128)(4,1)S(1)}, s32[]{:S(2)}) async-start(s8[7340032]{0:T(1024)(128)(4,1)} %bitcast.138), calls=%async_computation.7 | async-start | bytes 6291456
  106.0 4.0 %copy-start.2 = (bf16[64,36,2048]{2,1,0:T(8,128)(2,1)}, bf16[64,36,2048]{2,1,0:T(8,128)(2,1)S(1)}, u32[]{:S(2)}) copy-start(bf16[64,36,2048]{2,1,0:T(8,128)(2,1)S(1)} %copy_dynamic-update-slice_fusion.1) | copy-start | bytes 28311556
  122.1 30.9 %copy-start.5 = (bf16[1024,64]{0,1:T(8,128)(2,1)S(1)}, bf16[1024,64]{0,1:T(8,128)(2,1)}, u32[]{:S(2)}) copy-start(bf16[1024,64]{0,1:T(8,128)(2,1)} %param.15) | copy-start | bytes 393220
  122.1 30.9 %copy-start.6 = (bf16[1024,64]{0,1:T(8,128)(2,1)S(1)}, bf16[1024,64]{0,1:T(8,128)(2,1)}, u32[]{:S(2)}) copy-start(bf16[1024,64]{0,1:T(8,128)(2,1)} %param.16) | copy-start | bytes 393220
  152.9 9.5 %copy-start.3 = (bf16[1024,256]{1,0:T(8,128)(2,1)S(1)}, bf16[1024,256]{1,0:T(8,128)(2,1)}, u32[]{:S(2)}) copy-start(bf16[1024,256]{1,0:T(8,128)(2,1)} %param.14) | copy-start | bytes 1572868
  152.9 9.5 %copy-start.7 = (f32[4]{0:T(128)S(1)}, f32[4]{0:T(128)}, u32[]{:S(2)}) copy-start(f32[4]{0:T(128)} %param.17) | copy-start | bytes 52
  152.9 99.2 %reduce-scatter.3.cloned.1.call-start = ((), (), s32[]{:S(2)}) async-start(), calls=%async_computation.4 | async-start | bytes 5242880 | tf_op jit(solution)/shard_map/reduce_scatter | solution.py:122
  153.0 5.0 %collective-permute-start = (bf16[128,128]{0,1:T(8,128)(2,1)S(1)}, bf16[128,128]{0,1:T(8,128)(2,1)S(1)}, u32[]{:S(2)}, u32[]{:S(2)}) collective-permute-start(bf16[128,128]{0,1:T(8,128)(2,1)S(1)} %get-tuple-element.131), channel_id=1, source_target_pairs={{0,4},{4,8},{8,12},{12,16},{16,20},{20,24},{24,28},{1,5},{5,9},{9,... | collective-permute-start | bytes 98312 | tf_op jit(solution)/shard_map/ppermute | solution.py:44
  156.5 5.8 %collective-permute-start.1 = (bf16[128,128]{0,1:T(8,128)(2,1)S(1)}, bf16[128,128]{0,1:T(8,128)(2,1)S(1)}, u32[]{:S(2)}, u32[]{:S(2)}) collective-permute-start(bf16[128,128]{0,1:T(8,128)(2,1)S(1)} %get-tuple-element.132), channel_id=1, source_target_pairs={{4,0},{8,4},{12,8},{16,12},{20,16},{24,20},{28,24},{5,1},{9,5},{13... | collective-permute-start | bytes 98312 | tf_op jit(solution)/shard_map/ppermute | solution.py:45
  166.2 2.7 %copy-start.1 = (f32[768,512,4]{1,0,2:T(8,128)}, f32[768,512,4]{1,0,2:T(8,128)S(1)}, u32[]{:S(2)}) copy-start(f32[768,512,4]{1,0,2:T(8,128)S(1)} %get-tuple-element.182) | copy-start | bytes 18874372 | tf_op jit(solution)/shard_map/while
  179.1 2.7 %copy-start.1 = (f32[768,512,4]{1,0,2:T(8,128)}, f32[768,512,4]{1,0,2:T(8,128)S(1)}, u32[]{:S(2)}) copy-start(f32[768,512,4]{1,0,2:T(8,128)S(1)} %get-tuple-element.182) | copy-start | bytes 18874372 | tf_op jit(solution)/shard_map/while
  187.9 22.0 %copy-start.8 = (f32[128,2]{0,1:T(2,128)S(1)}, f32[128,2]{0,1:T(2,128)}, u32[]{:S(2)}) copy-start(f32[128,2]{0,1:T(2,128)} %param.22) | copy-start | bytes 3076
  204.4 36.8 %all-to-all-start.1 = ((bf16[8,36,2048]{2,1,0:T(8,128)(2,1)}), bf16[8,36,2048]{2,1,0:T(8,128)(2,1)}, u32[]{:S(2)}, u32[]{:S(2)}) async-start(bf16[8,36,2048]{2,1,0:T(8,128)(2,1)} %reduce-scatter.5.cloned.1.call-done), calls=%async_computation.3 | async-start | bytes 2621440 | tf_op jit(solution)/shard_map/all_to_all | solution.py:161
Sparse Core Ops, SparseCore 0:
  153.0 51.2 reduce-scatter.4
  207.5 44.5 reduce-scatter.2
